TPU v7x, 32 devices: a whole 2x2x4 slice. The times are simulated.
32 devices in a mesh: ep: 8 (over z, y), tp: 4 (over x, core).
Axes of the slice: x: 2, y: 2, z: 4, core: 2. Of those that a mesh axis runs over, the one named last changes fastest.
Arguments:
- tokens: bfloat16 [256, 2048], P('ep'), may hold values from -6 to 6
- gain_mix: bfloat16 [2048], replicated, may hold values from 0.099609375 to 1.8984375
- gain_ffn: bfloat16 [2048], replicated, may hold values from 0.099609375 to 1.8984375
- w_query: bfloat16 [2048, 1024], P('ep', 'tp'), may hold values from -0.125 to 0.125
- w_key: bfloat16 [2048, 1024], P('ep', 'tp'), may hold values from -0.125 to 0.125
- w_value: bfloat16 [2048, 1024], P('ep', 'tp'), may hold values from -0.125 to 0.125
- w_outgate: bfloat16 [2048, 1024], P('ep', 'tp'), may hold values from -0.125 to 0.125
- w_ingate: bfloat16 [2048, 8], replicated, may hold values from -0.125 to 0.125
- w_forget: bfloat16 [2048, 8], replicated, may hold values from -0.125 to 0.125
- bias_in: float32 [8], replicated, may hold values from -2 to 2
- bias_forget: float32 [8], replicated, may hold values from -1 to 3
- w_proj: bfloat16 [1024, 2048], P('tp'), may hold values from -0.1875 to 0.1875
- matrix_state: float32 [256, 8, 128, 128], P('ep', 'tp'), may hold values from -0.6 to 0.6
- normal_state: float32 [256, 8, 128], P('ep', 'tp'), may hold values from -0.6 to 0.6
- stab_state: float32 [256, 8], P('ep', 'tp'), may hold values from -1 to 1
- route_ids: int32 [256, 2], P('ep'), may hold values from 0 to 3, all different within a row; in each aligned block of 32 rows (0 to 31, 32 to 63, ...) at most 32 rows name the same one
- route_weights: float32 [256, 2], P('ep'), may hold values from 0.1 to 1
- w_exp_gate: bfloat16 [8, 2048, 1536], P('ep', None, 'tp'), may hold values from -0.125 to 0.125
- w_exp_up: bfloat16 [8, 2048, 1536], P('ep', None, 'tp'), may hold values from -0.125 to 0.125
- w_exp_down: bfloat16 [8, 1536, 2048], P('ep', 'tp'), may hold values from -0.109375 to 0.109375
Outputs:
- mixed_out: bfloat16 [256, 2048], P('ep', 'tp')
- matrix_out: float32 [256, 8, 128, 128], P('ep', 'tp')
- normal_out: float32 [256, 8, 128], P('ep', 'tp')
- stab_out: float32 [256, 8], P('ep', 'tp')
Inputs may be any that keep to these rules, and one draw needn't show every extreme that they name: `route_ids`: each row names 2 different experts; among the rows of one index of ep no expert is named by more than 32 rows, and in every draw some expert is named by exactly 32 of them.
All inputs are finite; a program needn't handle non-finite values.
Results may differ from a plain program's by a relative error of at most 0.015.
Values may be sent and summed in bfloat16 or wider, within the bound.
No kernel may reach another device: no remote copies, remote signals or barrier semaphores. Data moves between devices by JAX's collectives and lax.ppermute only.
A program may use at most 64 MiB of HBM per device.

v0:
```python
import jax
import jax.numpy as jnp
from jax import lax
from jax.sharding import PartitionSpec as P

norm_epsilon = 1e-06


def rms_scale(row_block, gain):
    wide = row_block.astype(jnp.float32)
    factor = lax.rsqrt(jnp.mean(wide * wide, axis=-1, keepdims=True) + norm_epsilon)
    return (wide * factor * gain.astype(jnp.float32)).astype(jnp.bfloat16)


def memory_step(
    query,
    key_rows,
    value_rows,
    gate_rows,
    in_pre,
    forget_pre,
    matrix_state,
    normal_state,
    stab_state,
):
    log_forget = jax.nn.log_sigmoid(forget_pre)
    stab_new = jnp.maximum(log_forget + stab_state, in_pre)
    carry = jnp.exp(log_forget + stab_state - stab_new)
    inflow = jnp.exp(in_pre - stab_new)
    scaled_keys = key_rows.astype(jnp.float32) * query.shape[-1] ** (-0.5)
    value_wide = value_rows.astype(jnp.float32)
    matrix_new = (
        carry[..., None, None] * matrix_state
        + inflow[..., None, None] * scaled_keys[..., :, None] * value_wide[..., None, :]
    )
    normal_new = carry[..., None] * normal_state + inflow[..., None] * scaled_keys
    query_wide = query.astype(jnp.float32)
    numer = jnp.einsum("shd,shde->she", query_wide, matrix_new, precision=lax.Precision.HIGHEST)
    denom = jnp.maximum(jnp.abs(jnp.sum(query_wide * normal_new, axis=-1)), 1.0)
    hidden = numer / denom[..., None] * jax.nn.sigmoid(gate_rows.astype(jnp.float32))
    return (hidden, matrix_new, normal_new, stab_new)


def dispatch_table(route_ids, experts, capacity):
    flat_ids = route_ids.reshape(-1)
    expert_hot = (flat_ids[:, None] == jnp.arange(experts, dtype=jnp.int32)[None, :]).astype(
        jnp.int32
    )
    slot_rank = jnp.sum((jnp.cumsum(expert_hot, axis=0) - 1) * expert_hot, axis=1)
    slot_hot = (slot_rank[:, None] == jnp.arange(capacity, dtype=jnp.int32)[None, :]).astype(
        jnp.float32
    )
    table = expert_hot.astype(jnp.float32)[:, :, None] * slot_hot[:, None, :]
    return table.reshape(flat_ids.shape[0], experts * capacity)


def send_rows(table, row_block, top_count, experts, capacity):
    repeated = jnp.repeat(row_block, top_count, axis=0)
    packed = jnp.einsum(
        "as,aw->sw", table.astype(jnp.bfloat16), repeated, preferred_element_type=jnp.float32
    ).astype(jnp.bfloat16)
    row_width = row_block.shape[1]
    doubled = jnp.broadcast_to(
        packed.reshape(experts, 1, capacity, row_width), (experts, 2, capacity, row_width)
    )
    return doubled.reshape(experts * 2 * capacity, row_width)


def body(
    tokens,
    gain_mix,
    gain_ffn,
    w_query,
    w_key,
    w_value,
    w_outgate,
    w_ingate,
    w_forget,
    bias_in,
    bias_forget,
    w_proj,
    matrix_state,
    normal_state,
    stab_state,
    route_ids,
    route_weights,
    w_exp_gate,
    w_exp_up,
    w_exp_down,
):
    ep_count = lax.axis_size("ep")
    tp_count = lax.axis_size("tp")
    tp_index = lax.axis_index("tp")
    seq_dev = tokens.shape[0]
    model_width = tokens.shape[1]
    heads_dev = matrix_state.shape[1]
    head_dim = matrix_state.shape[2]
    head_cols = w_query.shape[1]
    top_count = route_ids.shape[1]
    experts = ep_count // 2
    capacity = min(seq_dev, max(2, 2 * seq_dev * top_count // experts))
    col_width = model_width // tp_count
    normed = rms_scale(tokens, gain_mix)
    foreign = lax.all_to_all(normed, "ep", split_axis=1, concat_axis=0, tiled=True)
    summed = lax.psum_scatter(
        jnp.concatenate(
            [
                jnp.dot(foreign, weight, preferred_element_type=jnp.float32)
                for weight in (w_query, w_key, w_value, w_outgate)
            ],
            axis=1,
        ),
        "ep",
        scatter_dimension=0,
        tiled=True,
    )
    partials = [summed[:, offset * head_cols : (offset + 1) * head_cols] for offset in range(4)]
    query, key_rows, value_rows, gate_rows = [
        partial_value.astype(jnp.bfloat16).reshape(seq_dev, heads_dev, head_dim)
        for partial_value in partials
    ]
    head_first = tp_index * heads_dev
    in_pre = lax.dynamic_slice_in_dim(
        jnp.dot(normed, w_ingate, preferred_element_type=jnp.float32) + bias_in,
        head_first,
        heads_dev,
        1,
    )
    forget_pre = lax.dynamic_slice_in_dim(
        jnp.dot(normed, w_forget, preferred_element_type=jnp.float32) + bias_forget,
        head_first,
        heads_dev,
        1,
    )
    hidden, matrix_new, normal_new, stab_new = memory_step(
        query,
        key_rows,
        value_rows,
        gate_rows,
        in_pre,
        forget_pre,
        matrix_state,
        normal_state,
        stab_state,
    )
    cell = hidden.reshape(seq_dev, head_cols).astype(jnp.bfloat16)
    partial_out = jnp.dot(cell, w_proj, preferred_element_type=jnp.float32)
    table = dispatch_table(route_ids, experts, capacity)
    gate_local = w_exp_gate[0]
    up_local = w_exp_up[0]
    attended = lax.psum(partial_out.astype(jnp.bfloat16), "tp").astype(jnp.float32)
    resid = (tokens.astype(jnp.float32) + attended).astype(jnp.bfloat16)
    normed_ffn = rms_scale(resid, gain_ffn)
    own_resid = lax.dynamic_slice_in_dim(resid, tp_index * col_width, col_width, 1)
    outgoing = send_rows(table, normed_ffn, top_count, experts, capacity)
    received = lax.all_to_all(outgoing, "ep", split_axis=0, concat_axis=0, tiled=True)
    gate_sum = jnp.dot(received, gate_local, preferred_element_type=jnp.float32)
    up_sum = jnp.dot(received, up_local, preferred_element_type=jnp.float32)
    inner = (jax.nn.silu(gate_sum) * up_sum).astype(jnp.bfloat16)
    expert_terms = jnp.dot(inner, w_exp_down[0], preferred_element_type=jnp.float32)
    half_share = lax.psum_scatter(
        expert_terms.astype(jnp.bfloat16), "tp", scatter_dimension=1, tiled=True
    )
    returned = lax.all_to_all(half_share, "ep", split_axis=0, concat_axis=0, tiled=True)
    halves_summed = jnp.sum(
        returned.astype(jnp.float32).reshape(experts, 2, capacity, col_width), axis=1
    ).reshape(experts * capacity, col_width)
    weights = route_weights / jnp.sum(route_weights, axis=-1, keepdims=True)
    combine = jnp.sum(
        (table * weights.reshape(-1)[:, None]).reshape(seq_dev, top_count, experts * capacity),
        axis=1,
    )
    routed = jnp.dot(combine, halves_summed, precision=lax.Precision.HIGHEST)
    mixed_out = (own_resid.astype(jnp.float32) + routed).astype(jnp.bfloat16)
    return (mixed_out, matrix_new, normal_new, stab_new)


def solution(mesh):
    placed = (
        P("ep", None),
        P(),
        P(),
        P("ep", "tp"),
        P("ep", "tp"),
        P("ep", "tp"),
        P("ep", "tp"),
        P(),
        P(),
        P(),
        P(),
        P("tp", None),
        P("ep", "tp", None, None),
        P("ep", "tp", None),
        P("ep", "tp"),
        P("ep", None),
        P("ep", None),
        P("ep", None, "tp"),
        P("ep", None, "tp"),
        P("ep", "tp", None),
    )
    return jax.shard_map(
        body,
        mesh=mesh,
        in_specs=placed,
        out_specs=(P("ep", "tp"), P("ep", "tp", None, None), P("ep", "tp", None), P("ep", "tp")),
        check_vma=False,
    )
```

profile of v0, /device:TPU:0, one launch (start us, length us, event | category | flops | bytes accessed | tf_op | source)
XLA Modules:
  0.0 213.6 jit_solution(9406941949861868896)
XLA Ops:
  7.2 1.2 fusion.22
  8.4 0.7 convert_element_type.121
  9.1 1.0 fusion.24
  10.1 14.5 %all_to_all.40 = bf16[32,8,256]{2,0,1:T(8,128)(2,1)S(1)} all-to-all(bf16[32,8,256]{2,0,1:T(8,128)(2,1)S(1)} %bitcast.72), channel_id=1, replica_groups=mesh['ep'=8,'tp'=4] {'ep'}, dimensions={1} | all-to-all | bytes 262144 | tf_op jit(solution)/shard_map/all_to_all | solution.py:104
  24.6 1.1 fusion.41
  25.7 1.1 fusion.40
  26.9 0.2 fusion.39
  27.1 0.2 fusion.38
  27.5 1.3 copy.72
  30.1 61.5 %reduce-scatter.7.cloned.1.call-done = f32[32,1024]{1,0:T(8,128)} async-done(((f32[256,1024]{1,0:T(8,128)}), f32[32,1024]{1,0:T(8,128)}) %reduce-scatter.7.cloned.1.call-update) | async-done | bytes 131088
  91.6 1.1 copy.73
  93.1 0.8 multiply_reduce_fusion.2
  94.0 6.0 %multiply_reduce_fusion = (f32[32,2,128]{2,1,0:T(2,128)S(1)}, f32[32,2,128,128]{3,2,1,0:T(8,128)}) fusion(f32[32,2,128]{2,1,0:T(2,128)S(1)} %copy.74, f32[32,2,128]{2,1,0:T(2,128)S(1)} %copy.59, f32[32,2,128]{2,1,0:T(2,128)S(1)} %get-tuple-element.8, f32[32,2,128,128]{3,2,1,0:T(8,128)} %param.32, f32[32,2]{1,0:T(8,128)S(1)} %copy.56), kind=kLoop, calls=%fused_computation | loop fusion | flops 5234688 | bytes 8519936
  100.1 1.0 convolution_convert_fusion.2
  101.2 30.9 %all-reduce.2.cloned.1.call-done = bf16[32,2048]{1,0:T(8,128)(2,1)} async-done(((bf16[32,2048]{1,0:T(8,128)(2,1)}), bf16[32,2048]{1,0:T(8,128)(2,1)}) %all-reduce.2.cloned.1.call-update) | async-done | bytes 131088 | tf_op jit(solution)/shard_map/psum | solution.py:151
  132.1 1.1 fusion.19
  133.5 0.3 convolution_convert_fusion.1
  133.9 30.2 %all_to_all.41 = bf16[8,32,2048]{2,1,0:T(8,128)(2,1)S(1)} all-to-all(bf16[8,32,2048]{2,1,0:T(8,128)(2,1)S(1)} %bitcast.61), channel_id=1, replica_groups=mesh['ep'=8,'tp'=4] {'ep'}, dimensions={0} | all-to-all | bytes 2097152 | tf_op jit(solution)/shard_map/all_to_all | solution.py:156
  164.1 0.7 fusion.3
  164.9 3.7 %convolution_convert_fusion = bf16[256,2048]{1,0:T(8,128)(2,1)} fusion(bf16[1,384,2048]{2,1,0:T(8,128)(2,1)S(1)} %copy-done, bf16[256,2048]{1,0:T(8,128)(2,1)S(1)} %bitcast.60, bf16[1,2048,384]{2,1,0:T(8,128)(2,1)} %param.38, f32[256,384]{1,0:T(8,128)S(1)} %fusion.3), kind=kOutput, calls=%fused_computation.2 | convolution fusion | flops 806420480 | bytes 5636096 | tf_op jit(solution)/shard_map/dot_general | solution.py:160
  168.6 23.2 %reduce-scatter.5.cloned.1.call-done = bf16[256,512]{1,0:T(8,128)(2,1)} async-done(((bf16[256,2048]{1,0:T(8,128)(2,1)}), bf16[256,512]{1,0:T(8,128)(2,1)}) %reduce-scatter.5.cloned.1.call-update) | async-done | bytes 262160 | tf_op jit(solution)/shard_map/reduce_scatter | solution.py:161
  191.8 5.5 %all-to-all-start.2 = ((bf16[8,32,512]{2,1,0:T(8,128)(2,1)}), bf16[8,32,512]{2,1,0:T(8,128)(2,1)S(1)}, u32[]{:S(2)}, u32[]{:S(2)}) async-start(bf16[8,32,512]{2,1,0:T(8,128)(2,1)} %bitcast.74), calls=%async_computation.3 | async-start | bytes 524288 | tf_op jit(solution)/shard_map/all_to_all | solution.py:164
  197.8 8.3 %all-to-all-done.2 = bf16[8,32,512]{2,1,0:T(8,128)(2,1)S(1)} async-done(((bf16[8,32,512]{2,1,0:T(8,128)(2,1)}), bf16[8,32,512]{2,1,0:T(8,128)(2,1)S(1)}, u32[]{:S(2)}, u32[]{:S(2)}) %all-to-all-start.2) | async-done | bytes 262176 | tf_op jit(solution)/shard_map/all_to_all | solution.py:164
  206.2 0.9 fusion.13
  (78 shorter events, 3.0 us)
Async XLA Ops:
  7.2 157.7 %copy-start = (bf16[1,384,2048]{2,1,0:T(8,128)(2,1)S(1)}, bf16[1,384,2048]{2,1,0:T(8,128)(2,1)}, u32[]{:S(2)}) copy-start(bf16[1,384,2048]{2,1,0:T(8,128)(2,1)} %param.39) | copy-start | bytes 4718596
  7.2 19.7 %copy-start.4 = (bf16[256,256]{1,0:T(8,128)(2,1)S(1)}, bf16[256,256]{1,0:T(8,128)(2,1)}, u32[]{:S(2)}) copy-start(bf16[256,256]{1,0:T(8,128)(2,1)} %param.24) | copy-start | bytes 393220
  7.2 19.9 %copy-start.5 = (bf16[256,256]{1,0:T(8,128)(2,1)S(1)}, bf16[256,256]{1,0:T(8,128)(2,1)}, u32[]{:S(2)}) copy-start(bf16[256,256]{1,0:T(8,128)(2,1)} %param.23) | copy-start | bytes 393220
  7.2 84.4 %reduce-scatter.7.cloned.1.call-start = ((), (), s32[]{:S(2)}) async-start(), calls=%async_computation.7 | async-start | bytes 1179648
  27.4 1.5 copy-start.10
  27.4 1.9 copy-start.12
  27.4 1.9 copy-start.14
  27.5 2.0 copy-start.13
  27.5 2.0 copy-start.15
  27.5 2.2 %copy-start.11 = (f32[32,2]{0,1:T(2,128)S(1)}, f32[32,2]{0,1:T(2,128)}, u32[]{:S(2)}) copy-start(f32[32,2]{0,1:T(2,128)} %param.34) | copy-start | bytes 772
  28.8 64.3 %copy-start.6 = (f32[32,2,128]{2,1,0:T(2,128)S(1)}, f32[32,2,128]{2,1,0:T(2,128)}, u32[]{:S(2)}) copy-start(f32[32,2,128]{2,1,0:T(2,128)} %param.33) | copy-start | bytes 98308
  28.8 103.2 %all-reduce.2.cloned.1.call-start = ((), (), s32[]{:S(2)}) async-start(), calls=%async_computation.5 | async-start | bytes 262144 | tf_op jit(solution)/shard_map/psum | solution.py:151
  29.7 70.2 %copy-start.9 = (f32[32,2]{0,1:T(2,128)}, f32[32,2]{0,1:T(2,128)S(1)}, u32[]{:S(2)}) copy-start(f32[32,2]{0,1:T(2,128)S(1)} %get-tuple-element.12) | copy-start | bytes 772
  94.0 6.1 %copy-start.3 = (bf16[256,2048]{1,0:T(8,128)(2,1)S(1)}, bf16[256,2048]{1,0:T(8,128)(2,1)}, u32[]{:S(2)}) copy-start(bf16[256,2048]{1,0:T(8,128)(2,1)} %param.31) | copy-start | bytes 3145732
  99.9 1.2 copy-start.7
  100.0 32.1 %copy-start.2 = (bf16[32,2048]{1,0:T(8,128)(2,1)S(1)}, bf16[32,2048]{1,0:T(8,128)(2,1)}, u32[]{:S(2)}) copy-start(bf16[32,2048]{1,0:T(8,128)(2,1)} %param.20) | copy-start | bytes 393220
  101.1 90.7 %reduce-scatter.5.cloned.1.call-start = ((), (), s32[]{:S(2)}) async-start(), calls=%async_computation.6 | async-start | bytes 1310720 | tf_op jit(solution)/shard_map/reduce_scatter | solution.py:161
  133.8 30.3 %copy-start.1 = (bf16[1,2048,384]{2,1,0:T(8,128)(2,1)S(1)}, bf16[1,2048,384]{2,1,0:T(8,128)(2,1)}, u32[]{:S(2)}) copy-start(bf16[1,2048,384]{2,1,0:T(8,128)(2,1)} %param.37) | copy-start | bytes 4718596
  168.6 28.7 %copy-start.8 = (f32[32,2]{0,1:T(2,128)S(1)}, f32[32,2]{0,1:T(2,128)}, u32[]{:S(2)}) copy-start(f32[32,2]{0,1:T(2,128)} %param.36) | copy-start | bytes 772
  191.8 14.3 %all-to-all-start.2 = ((bf16[8,32,512]{2,1,0:T(8,128)(2,1)}), bf16[8,32,512]{2,1,0:T(8,128)(2,1)S(1)}, u32[]{:S(2)}, u32[]{:S(2)}) async-start(bf16[8,32,512]{2,1,0:T(8,128)(2,1)} %bitcast.74), calls=%async_computation.3 | async-start | bytes 524288 | tf_op jit(solution)/shard_map/all_to_all | solution.py:164
Sparse Core Ops, SparseCore 0:
  29.0 62.5 reduce-scatter.6
  101.2 30.8 all-reduce.1
  168.8 23.0 reduce-scatter.4
where the time goes:
time: 214 us
  waiting for transfers between devices  124 us (58%)
  blocking collectives  44.6 us (21%)
  between operations  14.2 us (7%)
  other arithmetic  11.5 us (5%)
  matrix products  9.5 us (4%)
  starting transfers between devices  5.62 us (3%)
  local copies, waits for them, and re-layouts  4.18 us (2%)
    unnamed x4, waiting for transfers between devices  61.5 us
    psum x1, waiting for transfers between devices, body(): lax.psum(partial_out.astype(jnp.bfloat16), 'tp').astype(jnp.float32)  30.9 us
    all_to_all x1, blocking collectives, body(): lax.all_to_all(outgoing, 'ep', split_axis=0, concat_axis=0, tiled=True)  30.2 us
    reduce_scatter x1, waiting for transfers between devices, body(): lax.psum_scatter(expert_terms.astype(jnp.bfloat16), 'tp', scatter_dimensi...  23.2 us
    all_to_all x1, blocking collectives, body(): lax.all_to_all(normed, 'ep', split_axis=1, concat_axis=0, tiled=True)  14.5 us
    all_to_all x1, waiting for transfers between devices, body(): lax.all_to_all(half_share, 'ep', split_axis=0, concat_axis=0, tiled=True)  8.28 us
    unnamed x1, other arithmetic  5.95 us
    all_to_all x1, starting transfers between devices, body(): lax.all_to_all(half_share, 'ep', split_axis=0, concat_axis=0, tiled=True)  5.5 us
  transfers between devices with their start and end apart: 4, of which 4 were waited for; matrix products, arithmetic and copies ran while one was open for 1% of the time, Pallas kernels for 0%

commit v1 on v0

--- a/solution.py
+++ b/solution.py
@@ -4,6 +4,11 @@
 from jax.sharding import PartitionSpec as P
 
 norm_epsilon = 1e-06
+
+
+def _get_tiles(piece_in):
+    piece_now = jnp.sum(jax.lax.all_gather(piece_in, "tp"), axis=0)
+    return piece_now
 
 
 def rms_scale(row_block, gain):
@@ -148,7 +153,7 @@
     table = dispatch_table(route_ids, experts, capacity)
     gate_local = w_exp_gate[0]
     up_local = w_exp_up[0]
-    attended = lax.psum(partial_out.astype(jnp.bfloat16), "tp").astype(jnp.float32)
+    attended = _get_tiles(partial_out.astype(jnp.bfloat16)).astype(jnp.float32)
     resid = (tokens.astype(jnp.float32) + attended).astype(jnp.bfloat16)
     normed_ffn = rms_scale(resid, gain_ffn)
     own_resid = lax.dynamic_slice_in_dim(resid, tp_index * col_width, col_width, 1)

time: 214 us -> 189 us (0.88)
  waiting for transfers between devices: 124 us -> 93.1 us
  blocking collectives: 44.6 us -> 51.4 us
    psum x1 -> x0, waiting for transfers between devices: 30.9 us -> none  [body(): lax.psum(partial_out.astype(jnp.bfloat16), 'tp').astype(jnp.float32)]
    all_gather x0 -> x1, blocking collectives: none -> 7.15 us  [_get_tiles(): piece_now = jnp.sum(jax.lax.all_gather(piece_in, 'tp'), axis=0)]
    unnamed x4 -> x3, waiting for transfers between devices: 61.5 us -> 61.5 us
  transfers between devices with their start and end apart: 4 -> 3, of which waited for: 4 -> 3; matrix products, arithmetic and copies ran while one was open for 1% -> 1% of each run, Pallas kernels for 0% -> 0%
where the time goes in v1:
time: 189 us; the launch traced here: 188 us
  waiting for transfers between devices  93.1 us (49%)
  blocking collectives  51.4 us (27%)
  between operations  14.5 us (8%)
  other arithmetic  10.7 us (6%)
  matrix products  8.88 us (5%)
  starting transfers between devices  5.62 us (3%)
  local copies, waits for them, and re-layouts  4.18 us (2%)
    unnamed x3, waiting for transfers between devices  61.5 us
    all_to_all x1, blocking collectives, body(): lax.all_to_all(outgoing, 'ep', split_axis=0, concat_axis=0, tiled=True)  29.8 us
    reduce_scatter x1, waiting for transfers between devices, body(): lax.psum_scatter(expert_terms.astype(jnp.bfloat16), 'tp', scatter_dimensi...  23.3 us
    all_to_all x1, blocking collectives, body(): lax.all_to_all(normed, 'ep', split_axis=1, concat_axis=0, tiled=True)  14.5 us
    all_to_all x1, waiting for transfers between devices, body(): lax.all_to_all(half_share, 'ep', split_axis=0, concat_axis=0, tiled=True)  8.24 us
    all_gather x1, blocking collectives, _get_tiles(): piece_now = jnp.sum(jax.lax.all_gather(piece_in, 'tp'), axis=0)  7.15 us
    unnamed x1, other arithmetic  5.95 us
    all_to_all x1, starting transfers between devices, body(): lax.all_to_all(half_share, 'ep', split_axis=0, concat_axis=0, tiled=True)  5.54 us
  transfers between devices with their start and end apart: 3, of which 3 were waited for; matrix products, arithmetic and copies ran while one was open for 1% of the time, Pallas kernels for 0%

profile of v1, /device:TPU:0, one launch (start us, length us, event | category | flops | bytes accessed | tf_op | source)
XLA Modules:
  0.0 188.3 jit_solution(18349755467467145281)
XLA Ops:
  7.2 1.2 fusion.22
  8.4 0.7 convert_element_type.123
  9.1 1.0 fusion.24
  10.1 14.5 %all_to_all.40 = bf16[32,8,256]{2,0,1:T(8,128)(2,1)S(1)} all-to-all(bf16[32,8,256]{2,0,1:T(8,128)(2,1)S(1)} %bitcast.74), channel_id=1, replica_groups=mesh['ep'=8,'tp'=4] {'ep'}, dimensions={1} | all-to-all | bytes 262144 | tf_op jit(solution)/shard_map/all_to_all | solution.py:109
  24.6 1.1 fusion.41
  25.7 1.1 fusion.40
  26.9 0.2 fusion.39
  27.1 0.2 fusion.38
  27.5 1.3 copy.72
  29.9 0.2 select_reduce_fusion
  30.2 61.5 %reduce-scatter.7.cloned.1.call-done = f32[32,1024]{1,0:T(8,128)} async-done(((f32[256,1024]{1,0:T(8,128)}), f32[32,1024]{1,0:T(8,128)}) %reduce-scatter.7.cloned.1.call-update) | async-done | bytes 131088
  91.6 1.1 copy.73
  93.2 0.8 multiply_reduce_fusion.2
  94.0 6.0 %multiply_reduce_fusion = (f32[32,2,128]{2,1,0:T(2,128)S(1)}, f32[32,2,128,128]{3,2,1,0:T(8,128)}) fusion(f32[32,2,128]{2,1,0:T(2,128)S(1)} %copy.74, f32[32,2,128]{2,1,0:T(2,128)S(1)} %copy.59, f32[32,2,128]{2,1,0:T(2,128)S(1)} %get-tuple-element.8, f32[32,2,128,128]{3,2,1,0:T(8,128)} %param.32, f32[32,2]{1,0:T(8,128)S(1)} %copy.56), kind=kLoop, calls=%fused_computation | loop fusion | flops 5234688 | bytes 8519936
  100.1 0.3 convolution_convert_fusion.2
  100.4 7.1 %all-gather = bf16[128,2048]{1,0:T(8,128)(2,1)S(1)} all-gather(bf16[32,2048]{1,0:T(8,128)(2,1)S(1)} %convolution_convert_fusion.2), channel_id=2, replica_groups=mesh['ep'=8,'tp'=4] {'tp'}, dimensions={0}, use_global_device_ids=true | all-gather | bytes 655360 | tf_op jit(solution)/shard_map/all_gather | solution.py:10
  108.2 0.3 convolution_convert_fusion.1
  108.6 29.8 %all_to_all.41 = bf16[8,32,2048]{2,1,0:T(8,128)(2,1)S(1)} all-to-all(bf16[8,32,2048]{2,1,0:T(8,128)(2,1)S(1)} %bitcast.62), channel_id=1, replica_groups=mesh['ep'=8,'tp'=4] {'ep'}, dimensions={0} | all-to-all | bytes 2097152 | tf_op jit(solution)/shard_map/all_to_all | solution.py:161
  138.4 0.7 fusion.3
  139.2 3.8 %convolution_convert_fusion = bf16[256,2048]{1,0:T(8,128)(2,1)} fusion(bf16[1,384,2048]{2,1,0:T(8,128)(2,1)S(1)} %copy-done, bf16[256,2048]{1,0:T(8,128)(2,1)S(1)} %bitcast.61, bf16[1,2048,384]{2,1,0:T(8,128)(2,1)} %param.38, f32[256,384]{1,0:T(8,128)S(1)} %fusion.3), kind=kOutput, calls=%fused_computation.2 | convolution fusion | flops 806420480 | bytes 5636096 | tf_op jit(solution)/shard_map/dot_general | solution.py:165
  143.0 23.3 %reduce-scatter.5.cloned.1.call-done = bf16[256,512]{1,0:T(8,128)(2,1)} async-done(((bf16[256,2048]{1,0:T(8,128)(2,1)}), bf16[256,512]{1,0:T(8,128)(2,1)}) %reduce-scatter.5.cloned.1.call-update) | async-done | bytes 262160 | tf_op jit(solution)/shard_map/reduce_scatter | solution.py:166
  166.3 5.5 %all-to-all-start.2 = ((bf16[8,32,512]{2,1,0:T(8,128)(2,1)}), bf16[8,32,512]{2,1,0:T(8,128)(2,1)S(1)}, u32[]{:S(2)}, u32[]{:S(2)}) async-start(bf16[8,32,512]{2,1,0:T(8,128)(2,1)} %bitcast.76), calls=%async_computation.3 | async-start | bytes 524288 | tf_op jit(solution)/shard_map/all_to_all | solution.py:169
  172.3 8.2 %all-to-all-done.2 = bf16[8,32,512]{2,1,0:T(8,128)(2,1)S(1)} async-done(((bf16[8,32,512]{2,1,0:T(8,128)(2,1)}), bf16[8,32,512]{2,1,0:T(8,128)(2,1)S(1)}, u32[]{:S(2)}, u32[]{:S(2)}) %all-to-all-start.2) | async-done | bytes 262176 | tf_op jit(solution)/shard_map/all_to_all | solution.py:169
  180.6 0.9 fusion.13
  (77 shorter events, 3.0 us)
Async XLA Ops:
  7.2 132.0 %copy-start = (bf16[1,384,2048]{2,1,0:T(8,128)(2,1)S(1)}, bf16[1,384,2048]{2,1,0:T(8,128)(2,1)}, u32[]{:S(2)}) copy-start(bf16[1,384,2048]{2,1,0:T(8,128)(2,1)} %param.39) | copy-start | bytes 4718596
  7.2 19.7 %copy-start.4 = (bf16[256,256]{1,0:T(8,128)(2,1)S(1)}, bf16[256,256]{1,0:T(8,128)(2,1)}, u32[]{:S(2)}) copy-start(bf16[256,256]{1,0:T(8,128)(2,1)} %param.24) | copy-start | bytes 393220
  7.2 19.9 %copy-start.5 = (bf16[256,256]{1,0:T(8,128)(2,1)S(1)}, bf16[256,256]{1,0:T(8,128)(2,1)}, u32[]{:S(2)}) copy-start(bf16[256,256]{1,0:T(8,128)(2,1)} %param.23) | copy-start | bytes 393220
  7.2 84.4 %reduce-scatter.7.cloned.1.call-start = ((), (), s32[]{:S(2)}) async-start(), calls=%async_computation.6 | async-start | bytes 1179648
  27.4 1.5 copy-start.7
  27.4 1.5 copy-start.10
  27.5 1.9 %copy-start.12 = (bf16[2048,8]{0,1:T(8,128)(2,1)S(1)}, bf16[2048,8]{0,1:T(8,128)(2,1)}, u32[]{:S(2)}) copy-start(bf16[2048,8]{0,1:T(8,128)(2,1)} %param.27) | copy-start | bytes 98308
  27.5 1.9 %copy-start.14 = (f32[8]{0:T(128)S(1)}, f32[8]{0:T(128)}, u32[]{:S(2)}) copy-start(f32[8]{0:T(128)} %param.29) | copy-start | bytes 100
  27.5 2.1 %copy-start.13 = (bf16[2048,8]{0,1:T(8,128)(2,1)S(1)}, bf16[2048,8]{0,1:T(8,128)(2,1)}, u32[]{:S(2)}) copy-start(bf16[2048,8]{0,1:T(8,128)(2,1)} %param.28) | copy-start | bytes 98308
  27.5 2.1 %copy-start.15 = (f32[8]{0:T(128)S(1)}, f32[8]{0:T(128)}, u32[]{:S(2)}) copy-start(f32[8]{0:T(128)} %param.30) | copy-start | bytes 100
  27.5 2.2 %copy-start.11 = (f32[32,2]{0,1:T(2,128)S(1)}, f32[32,2]{0,1:T(2,128)}, u32[]{:S(2)}) copy-start(f32[32,2]{0,1:T(2,128)} %param.34) | copy-start | bytes 772
  28.8 64.3 %copy-start.6 = (f32[32,2,128]{2,1,0:T(2,128)S(1)}, f32[32,2,128]{2,1,0:T(2,128)}, u32[]{:S(2)}) copy-start(f32[32,2,128]{2,1,0:T(2,128)} %param.33) | copy-start | bytes 98308
  28.8 137.4 %reduce-scatter.5.cloned.1.call-start = ((), (), s32[]{:S(2)}) async-start(), calls=%async_computation.5 | async-start | bytes 1310720 | tf_op jit(solution)/shard_map/reduce_scatter | solution.py:166
  29.7 70.2 %copy-start.9 = (f32[32,2]{0,1:T(2,128)}, f32[32,2]{0,1:T(2,128)S(1)}, u32[]{:S(2)}) copy-start(f32[32,2]{0,1:T(2,128)S(1)} %get-tuple-element.12) | copy-start | bytes 772
  94.0 6.1 %copy-start.3 = (bf16[256,2048]{1,0:T(8,128)(2,1)S(1)}, bf16[256,2048]{1,0:T(8,128)(2,1)}, u32[]{:S(2)}) copy-start(bf16[256,2048]{1,0:T(8,128)(2,1)} %param.31) | copy-start | bytes 3145732
  100.0 7.7 %copy-start.2 = (bf16[32,2048]{1,0:T(8,128)(2,1)S(1)}, bf16[32,2048]{1,0:T(8,128)(2,1)}, u32[]{:S(2)}) copy-start(bf16[32,2048]{1,0:T(8,128)(2,1)} %param.20) | copy-start | bytes 393220
  108.5 29.9 %copy-start.1 = (bf16[1,2048,384]{2,1,0:T(8,128)(2,1)S(1)}, bf16[1,2048,384]{2,1,0:T(8,128)(2,1)}, u32[]{:S(2)}) copy-start(bf16[1,2048,384]{2,1,0:T(8,128)(2,1)} %param.37) | copy-start | bytes 4718596
  142.9 28.9 %copy-start.8 = (f32[32,2]{0,1:T(2,128)S(1)}, f32[32,2]{0,1:T(2,128)}, u32[]{:S(2)}) copy-start(f32[32,2]{0,1:T(2,128)} %param.36) | copy-start | bytes 772
  166.3 14.3 %all-to-all-start.2 = ((bf16[8,32,512]{2,1,0:T(8,128)(2,1)}), bf16[8,32,512]{2,1,0:T(8,128)(2,1)S(1)}, u32[]{:S(2)}, u32[]{:S(2)}) async-start(bf16[8,32,512]{2,1,0:T(8,128)(2,1)} %bitcast.76), calls=%async_computation.3 | async-start | bytes 524288 | tf_op jit(solution)/shard_map/all_to_all | solution.py:169
Sparse Core Ops, SparseCore 0:
  29.0 62.5 reduce-scatter.6
  143.1 23.1 reduce-scatter.4
